TPU v7x, 128 devices: a whole 4x4x4 slice. The times are simulated.
128 devices in a mesh: ep: 64 (over z, y, x), tp: 2 (over core).
Axes of the slice: x: 4, y: 4, z: 4, core: 2. Of those that a mesh axis runs over, the one named last changes fastest.
Arguments:
- tokens: bfloat16 [1024, 2048], P('ep'), may hold values from -6 to 6
- norm_gain: float32 [2048], replicated, may hold values from 0.1 to 1.9
- query_weight: bfloat16 [2048, 1024], P('ep', 'tp'), may hold values from -0.125 to 0.125
- key_weight: bfloat16 [2048, 1024], P('ep', 'tp'), may hold values from -0.125 to 0.125
- value_weight: bfloat16 [2048, 1024], P('ep', 'tp'), may hold values from -0.125 to 0.125
- outgate_weight: bfloat16 [2048, 1024], P('ep', 'tp'), may hold values from -0.125 to 0.125
- input_weight: bfloat16 [2048, 8], P('ep', 'tp'), may hold values from -0.125 to 0.125
- forget_weight: bfloat16 [2048, 8], P('ep', 'tp'), may hold values from -0.125 to 0.125
- forget_bias: float32 [8], P('tp'), may hold values from -1 to 5
- memory: float32 [1024, 8, 128, 128], P('ep', 'tp'), may hold values from -2.4 to 2.4
- stabilizer: float32 [1024, 8], P('ep', 'tp'), may hold values from -3 to 3
- head_gain: float32 [1024], P('tp'), may hold values from 0.1 to 1.9
- mix_weight: bfloat16 [1024, 2048], P('tp', 'ep'), may hold values from -0.1875 to 0.1875
- second_gain: float32 [2048], replicated, may hold values from 0.1 to 1.9
- route_experts: int32 [1024, 4], P('ep'), may hold values from 0 to 63, all different within a row; in each aligned block of 16 rows (0 to 15, 16 to 31, ...) at most 2 rows name the same one
- route_weight: float32 [1024, 4], P('ep'), may hold values from 0.1 to 1
- expert_gate: bfloat16 [64, 2048, 2048], P('ep', None, 'tp'), may hold values from -0.5 to 0.5
- expert_up: bfloat16 [64, 2048, 2048], P('ep', None, 'tp'), may hold values from -0.5 to 0.5
- expert_down: bfloat16 [64, 2048, 2048], P('ep', 'tp'), may hold values from -0.03125 to 0.03125
- dense_gate: bfloat16 [4096, 2048], P(('ep', 'tp')), may hold values from -0.125 to 0.125
- dense_up: bfloat16 [4096, 2048], P(('ep', 'tp')), may hold values from -0.125 to 0.125
- dense_down: bfloat16 [4096, 2048], P(('ep', 'tp')), may hold values from -0.09375 to 0.09375
- branch_scale: float32 [2048], replicated, may hold values from 0.3 to 1.5
Outputs:
- mixed: bfloat16 [1024, 2048], P('ep', 'tp')
- memory_new: float32 [1024, 8, 128, 128], P('ep', 'tp')
- stabilizer_new: float32 [1024, 8], P('ep', 'tp')
Inputs may be any that keep to these rules, and one draw needn't show every extreme that they name: `route_experts`: each row names 4 different experts. Within each aligned block of 16 rows no expert is named by more than 2 rows, and in every draw some expert is named by exactly 2 rows of some block.
All inputs are finite; a program needn't handle non-finite values.
Results may differ from a plain program's by a relative error of at most 0.03.
Values may be sent and summed in bfloat16 or wider, within the bound.
A program may use at most 128 MiB of HBM per device.

v0:
```python
import jax
import jax.numpy as jnp
from jax import lax
from jax.sharding import PartitionSpec as P

norm_eps = 1e-05
clamp_limit = 7.0
sigmoid_slope = 1.702


def in_one_piece(arrays, axis, dim, along):
    widths = [a.shape[along] for a in arrays]
    both = jnp.concatenate(arrays, axis=along)
    whole = lax.all_gather(both, axis, axis=dim, tiled=True)
    return tuple(jnp.split(whole, [sum(widths[:k]) for k in range(1, len(widths))], axis=along))


def sent_to_all(shard, axis):
    devices = lax.axis_size(axis)
    return lax.all_to_all(
        jnp.broadcast_to(shard[None], (devices, *shard.shape)), axis, 0, 0, tiled=True
    )


def taken_together(shard, axis):
    return sent_to_all(shard, axis).astype(jnp.float32).sum(axis=0)


def cut_along(shard, dim, devices):
    lengths = shard.shape
    pieces = shard.reshape(*lengths[:dim], devices, lengths[dim] // devices, *lengths[dim + 1 :])
    return jnp.moveaxis(pieces, dim, 0)


def sent_and_summed(shard, axis, dim):
    devices = lax.axis_size(axis)
    pieces = lax.all_to_all(cut_along(shard, dim, devices), axis, 0, 0, tiled=True)
    return jnp.sum(pieces.astype(jnp.float32), axis=0)


def rms_scale(values, gain):
    mean_square = jnp.mean(values * values, axis=-1, keepdims=True)
    return values * lax.rsqrt(mean_square + norm_eps) * gain


def round_half(values):
    return lax.optimization_barrier(values.astype(jnp.bfloat16)).astype(jnp.float32)


def clamped_unit(gate_pre, up_pre):
    gate_clamped = jnp.minimum(gate_pre, clamp_limit)
    up_clamped = jnp.clip(up_pre, -clamp_limit, clamp_limit)
    return (
        (up_clamped + 1.0) * gate_clamped * jax.nn.sigmoid(sigmoid_slope * gate_clamped)
    ).astype(jnp.bfloat16)


def memory_step(projected, forget_bias, memory, stabilizer, head_gain):
    query_rows, key_rows, value_rows, outgate_rows, input_pre, forget_pre = projected
    sequences, head_count = stabilizer.shape
    head_size = memory.shape[-1]
    log_forget = jax.nn.log_sigmoid(forget_pre + forget_bias)
    stab_new = jnp.maximum(log_forget + stabilizer, input_pre)
    carried = jnp.exp(log_forget + stabilizer - stab_new)
    written = jnp.exp(input_pre - stab_new)
    query_heads = query_rows.astype(jnp.float32).reshape(sequences, head_count, head_size)
    key_heads = key_rows.astype(jnp.float32).reshape(
        sequences, head_count, head_size
    ) * head_size ** (-0.5)
    value_heads = value_rows.astype(jnp.float32).reshape(sequences, head_count, head_size)
    memory_new = (
        carried[:, :, None, None] * memory
        + written[:, :, None, None] * value_heads[:, :, :, None] * key_heads[:, :, None, :]
    )
    readout = jnp.einsum("bhvk,bhk->bhv", memory_new, query_heads)
    out_gate = jax.nn.sigmoid(
        outgate_rows.astype(jnp.float32).reshape(sequences, head_count, head_size)
    )
    gated = (rms_scale(readout, head_gain.reshape(head_count, head_size)) * out_gate).astype(
        jnp.bfloat16
    )
    return (gated.reshape(sequences, head_count * head_size), memory_new, stab_new)


def expert_apply(rows, gate_weight, up_weight, down_weight):
    gate_pre = jnp.dot(rows, gate_weight, preferred_element_type=jnp.float32)
    up_pre = jnp.dot(rows, up_weight, preferred_element_type=jnp.float32)
    activity = clamped_unit(gate_pre, up_pre)
    return jnp.dot(activity, down_weight, preferred_element_type=jnp.float32).astype(jnp.bfloat16)


def slot_table(hit_mask, capacity):
    ranks = jnp.cumsum(hit_mask, axis=1) - 1.0
    slots = jnp.arange(capacity).astype(jnp.float32)
    return hit_mask[:, None, :] * (ranks[:, None, :] == slots[None, :, None]).astype(jnp.float32)


def body(
    tokens,
    norm_gain,
    query_weight,
    key_weight,
    value_weight,
    outgate_weight,
    input_weight,
    forget_weight,
    forget_bias,
    memory,
    stabilizer,
    head_gain,
    mix_weight,
    second_gain,
    route_experts,
    route_weight,
    expert_gate,
    expert_up,
    expert_down,
    dense_gate,
    dense_up,
    dense_down,
    branch_scale,
):
    sequences, model_width = tokens.shape
    ep_count = lax.axis_size("ep")
    tp_count = lax.axis_size("tp")
    part_width = model_width // tp_count
    top_count = route_experts.shape[1]
    expert_count = expert_gate.shape[0] * ep_count
    capacity = max(2, 2 * sequences * top_count // expert_count)
    inputs_float = tokens.astype(jnp.float32)
    normed = rms_scale(inputs_float, norm_gain).astype(jnp.bfloat16)
    pieces = in_one_piece(
        (query_weight, key_weight, value_weight, outgate_weight, input_weight, forget_weight),
        "ep",
        0,
        1,
    )
    sums = tuple((jnp.dot(normed, piece, preferred_element_type=jnp.float32) for piece in pieces))
    projected = (
        sums[0].astype(jnp.bfloat16),
        sums[1].astype(jnp.bfloat16),
        sums[2].astype(jnp.bfloat16),
        sums[3].astype(jnp.bfloat16),
        sums[4],
        sums[5],
    )
    gated, memory_new, stab_new = memory_step(projected, forget_bias, memory, stabilizer, head_gain)
    partial_value = jnp.dot(
        gated,
        lax.all_gather(mix_weight, "ep", axis=1, tiled=True),
        preferred_element_type=jnp.float32,
    )
    attended = taken_together(round_half(partial_value).astype(jnp.bfloat16), "tp").astype(
        jnp.float32
    )
    residual = (inputs_float + attended).astype(jnp.bfloat16)
    residual_float = residual.astype(jnp.float32)
    normed_second = rms_scale(residual_float, second_gain).astype(jnp.bfloat16)
    own_residual = lax.dynamic_slice_in_dim(
        residual_float, lax.axis_index("tp") * part_width, part_width, 1
    )
    own_scale = lax.dynamic_slice_in_dim(
        branch_scale, lax.axis_index("tp") * part_width, part_width, 0
    )
    matched = route_experts[:, :, None] == jnp.arange(expert_count)[None, None, :]
    hit_mask = jnp.any(matched, axis=1).astype(jnp.float32).T
    weights = jnp.sum(jnp.where(matched, route_weight[:, :, None], 0.0), axis=1).T
    select = slot_table(hit_mask, capacity)
    outgoing = jnp.einsum(
        "ecs,sd->ecd",
        select.astype(jnp.bfloat16),
        normed_second,
        preferred_element_type=jnp.float32,
    ).astype(jnp.bfloat16)
    received = lax.all_to_all(outgoing, "ep", split_axis=0, concat_axis=0, tiled=True)
    count = received.shape[1]
    partial_out = expert_apply(
        received.reshape(-1, model_width), expert_gate[0], expert_up[0], expert_down[0]
    )
    halves = sent_and_summed(partial_out.astype(jnp.float32).astype(jnp.bfloat16), "tp", 1)
    returned = lax.all_to_all(
        halves.reshape(ep_count, count, part_width).astype(jnp.bfloat16),
        "ep",
        split_axis=0,
        concat_axis=0,
        tiled=True,
    ).astype(jnp.float32)
    routed = jnp.einsum("ecs,ecd->sd", select * weights[:, None, :], returned)
    gate_piece, up_piece, down_piece = in_one_piece((dense_gate, dense_up, dense_down), "ep", 0, 1)
    gate_rows = jnp.einsum(
        "td,fd->tf", normed_second, gate_piece, preferred_element_type=jnp.float32
    )
    lift_rows = jnp.einsum("td,fd->tf", normed_second, up_piece, preferred_element_type=jnp.float32)
    activity = (jax.nn.silu(gate_rows) * lift_rows).astype(jnp.bfloat16)
    total = jnp.dot(activity, down_piece, preferred_element_type=jnp.float32)
    halves = sent_and_summed(total.astype(jnp.bfloat16), "tp", 1)
    branch = halves * own_scale
    mixed = own_residual + routed + branch
    return (mixed.astype(jnp.bfloat16), memory_new, stab_new)


def solution(mesh):
    in_specs = (
        P("ep", None),
        P(),
        P("ep", "tp"),
        P("ep", "tp"),
        P("ep", "tp"),
        P("ep", "tp"),
        P("ep", "tp"),
        P("ep", "tp"),
        P("tp"),
        P("ep", "tp", None, None),
        P("ep", "tp"),
        P("tp"),
        P("tp", "ep"),
        P(),
        P("ep", None),
        P("ep", None),
        P("ep", None, "tp"),
        P("ep", None, "tp"),
        P("ep", "tp", None),
        P(("ep", "tp"), None),
        P(("ep", "tp"), None),
        P(("ep", "tp"), None),
        P(),
    )
    out_specs = (P("ep", "tp"), P("ep", "tp", None, None), P("ep", "tp"))
    return jax.shard_map(body, mesh=mesh, in_specs=in_specs, out_specs=out_specs, check_vma=False)
```

profile of v0, /device:TPU:0, one launch (start us, length us, event | category | flops | bytes accessed | tf_op | source)
XLA Modules:
  0.0 342.2 jit_solution(8388457338373234706)
XLA Ops:
  7.2 0.8 copy.56
  8.0 0.8 copy.57
  8.8 1.5 concatenate.6
  10.4 0.7 all-gather.6.cloned.1.call-update
  11.2 1.8 pad_maximum_fusion
  13.0 0.8 fusion.119
  14.1 1.0 fusion.107
  15.1 78.9 %all-gather.4.cloned.1.call-done = bf16[2048,2056]{1,0:T(8,128)(2,1)} async-done(((bf16[32,2056]{1,0:T(8,128)(2,1)}), bf16[2048,2056]{1,0:T(8,128)(2,1)}) %all-gather.4.cloned.1.call-update) | async-done | bytes 8421392 | tf_op jit(solution)/shard_map/all_gather | solution.py:14
  94.0 1.3 fusion.94
  95.3 1.8 subtract_exponential_fusion.1
  97.2 2.1 fusion.58
  99.4 2.0 fusion.67
  101.4 2.0 fusion.70
  103.4 2.0 fusion.88
  105.6 3.1 multiply_add_fusion
  108.7 2.0 copy-done
  110.7 1.2 fusion.149
  112.1 49.8 %all-gather.6.cloned.1.call-done = bf16[512,2048]{0,1:T(8,128)(2,1)} async-done(((bf16[512,32]{0,1:T(8,128)(2,1)}), bf16[512,2048]{0,1:T(8,128)(2,1)}) %all-gather.6.cloned.1.call-update) | async-done | bytes 2097168 | tf_op jit(solution)/shard_map/all_gather | solution.py:150
  161.8 2.2 convolution_convert_fusion.1
  164.1 3.8 %all_to_all.25 = bf16[2,16,2048]{2,1,0:T(8,128)(2,1)S(1)} all-to-all(bf16[2,16,2048]{2,1,0:T(8,128)(2,1)S(1)} %broadcast_in_dim.10), channel_id=1, replica_groups=mesh['ep'=64,'tp'=2] {'tp'}, dimensions={0} | all-to-all | bytes 262144 | tf_op jit(solution)/shard_map/all_to_all | solution.py:20
  169.2 22.5 %all_to_all.26 = bf16[64,2,2048]{2,1,0:T(2,128)(2,1)S(1)} all-to-all(bf16[64,2,2048]{2,1,0:T(2,128)(2,1)S(1)} %copy.62), channel_id=1, replica_groups=mesh['ep'=64,'tp'=2] {'ep'}, dimensions={0} | all-to-all | bytes 1048576 | tf_op jit(solution)/shard_map/all_to_all | solution.py:175
  191.9 2.9 fusion.37
  194.8 5.5 %fusion.12 = bf16[128,2048]{1,0:T(8,128)(2,1)S(1)} fusion(bf16[1,1024,2048]{2,1,0:T(8,128)(2,1)} %param.41, f32[128,1024]{1,0:T(8,128)S(1)} %fusion.37, bf16[128,2048]{1,0:T(8,128)(2,1)S(1)} %reshape.97, bf16[1,2048,1024]{2,1,0:T(8,128)(2,1)} %param.40), kind=kOutput, calls=%fused_computation.13 | convolution fusion | flops 1075183616 | bytes 9961472 | tf_op jit(solution)/shard_map/dot_general | solution.py:89
  200.4 4.2 %all_to_all.27 = bf16[2,128,1024]{2,1,0:T(8,128)(2,1)S(1)} all-to-all(bf16[2,128,1024]{2,1,0:T(8,128)(2,1)S(1)} %bitcast.67), channel_id=1, replica_groups=mesh['ep'=64,'tp'=2] {'tp'}, dimensions={0} | all-to-all | bytes 1048576 | tf_op jit(solution)/shard_map/all_to_all | solution.py:37
  204.6 0.8 convert_element_type.114
  205.4 91.2 %all-gather.8.cloned.1.call-done = bf16[2048,6144]{1,0:T(8,128)(2,1)} async-done(((bf16[32,6144]{1,0:T(8,128)(2,1)}), bf16[2048,6144]{1,0:T(8,128)(2,1)}) %all-gather.8.cloned.1.call-update) | async-done | bytes 25165840 | tf_op jit(solution)/shard_map/all_gather | solution.py:14
  296.6 5.6 %fusion.4 = f32[16,2048]{1,0:T(8,128)S(1)} fusion(bf16[16,2048]{1,0:T(8,128)(2,1)S(1)} %multiply_convert_fusion, bf16[2048,6144]{1,0:T(8,128)(2,1)} %all-gather.8.cloned.1.call-done), kind=kOutput, calls=%fused_computation.4 | convolution fusion | flops 134217728 | bytes 8585216 | tf_op jit(solution)/shard_map/td,fd->tf/dot_general | solution.py:190
  302.3 9.2 %fusion.21 = bf16[16,2048]{1,0:T(8,128)(2,1)S(1)} fusion(bf16[2048,6144]{1,0:T(8,128)(2,1)} %all-gather.8.cloned.1.call-done, bf16[16,2048]{1,0:T(8,128)(2,1)S(1)} %multiply_convert_fusion, f32[16,2048]{1,0:T(8,128)S(1)} %fusion.4), kind=kOutput, calls=%fused_computation.17 | convolution fusion | flops 268664832 | bytes 17039360 | tf_op jit(solution)/shard_map/dot_general | solution.py:195
  311.5 3.8 %all_to_all.28 = bf16[2,16,1024]{2,1,0:T(8,128)(2,1)S(1)} all-to-all(bf16[2,16,1024]{2,1,0:T(8,128)(2,1)S(1)} %bitcast.71), channel_id=1, replica_groups=mesh['ep'=64,'tp'=2] {'tp'}, dimensions={0} | all-to-all | bytes 131072 | tf_op jit(solution)/shard_map/all_to_all | solution.py:37
  315.2 8.6 %all-to-all-start.3 = ((bf16[64,2,1024]{2,1,0:T(2,128)(2,1)}), bf16[64,2,1024]{2,1,0:T(2,128)(2,1)S(1)}, u32[]{:S(2)}, u32[]{:S(2)}) async-start(bf16[64,2,1024]{2,1,0:T(2,128)(2,1)} %convert_element_type.114), calls=%async_computation.3 | async-start | bytes 524288 | tf_op jit(solution)/shard_map/all_to_all | solution.py:181
  324.0 10.8 %all-to-all-done.3 = bf16[64,2,1024]{2,1,0:T(2,128)(2,1)S(1)} async-done(((bf16[64,2,1024]{2,1,0:T(2,128)(2,1)}), bf16[64,2,1024]{2,1,0:T(2,128)(2,1)S(1)}, u32[]{:S(2)}, u32[]{:S(2)}) %all-to-all-start.3) | async-done | bytes 262176 | tf_op jit(solution)/shard_map/all_to_all | solution.py:181
  334.8 0.9 fusion.54
  (54 shorter events, 2.7 us)
Async XLA Ops:
  7.2 92.2 %copy-start.1 = (bf16[16,2048]{1,0:T(8,128)(2,1)S(1)}, bf16[16,2048]{1,0:T(8,128)(2,1)}, u32[]{:S(2)}) copy-start(bf16[16,2048]{1,0:T(8,128)(2,1)} %param.23) | copy-start | bytes 196612
  7.2 92.2 %copy-start.8 = (f32[2048]{0:T(1024)S(1)}, f32[2048]{0:T(1024)}, u32[]{:S(2)}) copy-start(f32[2048]{0:T(1024)} %param.24) | copy-start | bytes 24580
  7.2 86.8 %all-gather.4.cloned.1.call-start = ((), (), s32[]{:S(2)}) async-start(), calls=%async_computation.5 | async-start | bytes 9052160 | tf_op jit(solution)/shard_map/all_gather | solution.py:14
  10.4 151.5 %all-gather.6.cloned.1.call-start = ((), (), s32[]{:S(2)}) async-start(), calls=%async_computation.6 | async-start | bytes 2129920 | tf_op jit(solution)/shard_map/all_gather | solution.py:150
  11.1 285.5 %all-gather.8.cloned.1.call-start = ((), (), s32[]{:S(2)}) async-start(), calls=%async_computation.7 | async-start | bytes 25559040 | tf_op jit(solution)/shard_map/all_gather | solution.py:14
  97.1 8.4 %copy-start.5 = (f32[16,4]{0,1:T(4,128)}, f32[16,4]{0,1:T(4,128)S(1)}, u32[]{:S(2)}) copy-start(f32[16,4]{0,1:T(4,128)S(1)} %get-tuple-element.6) | copy-start | bytes 772
  108.7 2.0 copy-start
  110.7 1.3 copy-start.4
  110.7 57.5 %copy-start.2 = (f32[2048]{0:T(1024)S(1)}, f32[2048]{0:T(1024)}, u32[]{:S(2)}) copy-start(f32[2048]{0:T(1024)} %param.36) | copy-start | bytes 24580
  302.2 21.6 %copy-start.6 = (f32[2048]{0:T(1024)S(1)}, f32[2048]{0:T(1024)}, u32[]{:S(2)}) copy-start(f32[2048]{0:T(1024)} %param.45) | copy-start | bytes 24580
  302.2 21.7 %copy-start.3 = (s32[16,4]{0,1:T(4,128)S(1)}, s32[16,4]{0,1:T(4,128)}, u32[]{:S(2)}) copy-start(s32[16,4]{0,1:T(4,128)} %param.37) | copy-start | bytes 772
  302.2 21.7 %copy-start.7 = (f32[16,4]{0,1:T(4,128)S(1)}, f32[16,4]{0,1:T(4,128)}, u32[]{:S(2)}) copy-start(f32[16,4]{0,1:T(4,128)} %param.38) | copy-start | bytes 772
  315.2 19.5 %all-to-all-start.3 = ((bf16[64,2,1024]{2,1,0:T(2,128)(2,1)}), bf16[64,2,1024]{2,1,0:T(2,128)(2,1)S(1)}, u32[]{:S(2)}, u32[]{:S(2)}) async-start(bf16[64,2,1024]{2,1,0:T(2,128)(2,1)} %convert_element_type.114), calls=%async_computation.3 | async-start | bytes 524288 | tf_op jit(solution)/shard_map/all_to_all | solution.py:181
Sparse Core Ops, SparseCore 0:
  11.3 82.5 all-gather.3
  96.8 64.9 all-gather.5
  164.6 131.9 all-gather.7
where the time goes:
time: 343 us; the launch traced here: 342 us
  waiting for transfers between devices  231 us (67%)
  matrix products  39.2 us (11%)
  blocking collectives  34.3 us (10%)
  between operations  14 us (4%)
  starting transfers between devices  8.72 us (3%)
  other arithmetic  7.55 us (2%)
  local copies, waits for them, and re-layouts  7.16 us (2%)
    all_gather x2, waiting for transfers between devices, in_one_piece(): whole = lax.all_gather(both, axis, axis=dim, tiled=True)  170 us
    all_gather x1, waiting for transfers between devices, body(): lax.all_gather(mix_weight, 'ep', axis=1, tiled=True)  49.8 us
    all_to_all x1, blocking collectives, body(): lax.all_to_all(outgoing, 'ep', split_axis=0, concat_axis=0, tiled=True)  22.5 us
    dot_general x6, matrix products, body(): jnp.dot(normed, piece, preferred_element_type=jnp.float32)  11.2 us
    all_to_all x1, waiting for transfers between devices, body(): lax.all_to_all(halves.reshape(ep_count, count, part_width).astype(jnp.bfl...  10.8 us
    dot_general x1, matrix products, body(): total = jnp.dot(activity, down_piece, preferred_element_type=jnp.float32)  9.18 us
    all_to_all x1, starting transfers between devices, body(): lax.all_to_all(halves.reshape(ep_count, count, part_width).astype(jnp.bfl...  8.6 us
    all_to_all x2, blocking collectives, sent_and_summed(): lax.all_to_all(cut_along(shard, dim, devices), axis, 0, 0, tiled=True)  7.95 us
  transfers between devices with their start and end apart: 4, of which 4 were waited for; matrix products, arithmetic and copies ran while one was open for 10% of the time, Pallas kernels for 0%

commit v1 on v0

--- a/solution.py
+++ b/solution.py
@@ -147,7 +147,9 @@
     gated, memory_new, stab_new = memory_step(projected, forget_bias, memory, stabilizer, head_gain)
     partial_value = jnp.dot(
         gated,
-        lax.all_gather(mix_weight, "ep", axis=1, tiled=True),
+        jnp.concatenate(
+            lax.all_to_all(jnp.stack([mix_weight] * lax.axis_size("ep")), "ep", 0, 0), axis=1
+        ),
         preferred_element_type=jnp.float32,
     )
     attended = taken_together(round_half(partial_value).astype(jnp.bfloat16), "tp").astype(

time: 343 us -> 295 us (0.86)
  waiting for transfers between devices: 231 us -> 169 us
  starting transfers between devices: 8.72 us -> 20.2 us
  blocking collectives: 34.3 us -> 38.1 us
    all_gather x1 -> x0, waiting for transfers between devices: 49.8 us -> none  [body(): lax.all_gather(mix_weight, 'ep', axis=1, tiled=True)]
    all_gather x2, waiting for transfers between devices: 170 us -> 158 us  [in_one_piece(): whole = lax.all_gather(both, axis, axis=dim, tiled=True)]
    all_to_all x0 -> x1, starting transfers between devices: none -> 11.5 us  [body(): lax.all_to_all(jnp.stack([mix_weight] * lax.axis_size('ep')), 'ep', 0, 0)]
    all_to_all x1, blocking collectives: 22.5 us -> 26.4 us  [body(): lax.all_to_all(outgoing, 'ep', split_axis=0, concat_axis=0, tiled=True)]
  transfers between devices with their start and end apart: 4 -> 4, of which waited for: 4 -> 3; matrix products, arithmetic and copies ran while one was open for 10% -> 11% of each run, Pallas kernels for 0% -> 0%
where the time goes in v1:
time: 295 us; the launch traced here: 294 us
  waiting for transfers between devices  169 us (57%)
  blocking collectives  38.1 us (13%)
  matrix products  37 us (13%)
  starting transfers between devices  20.2 us (7%)
  between operations  14.4 us (5%)
  local copies, waits for them, and re-layouts  9.45 us (3%)
  other arithmetic  6.15 us (2%)
    all_gather x2, waiting for transfers between devices, in_one_piece(): whole = lax.all_gather(both, axis, axis=dim, tiled=True)  158 us
    all_to_all x1, blocking collectives, body(): lax.all_to_all(outgoing, 'ep', split_axis=0, concat_axis=0, tiled=True)  26.4 us
    all_to_all x1, starting transfers between devices, body(): lax.all_to_all(jnp.stack([mix_weight] * lax.axis_size('ep')), 'ep', 0, 0)  11.5 us
    dot_general x6, matrix products, body(): jnp.dot(normed, piece, preferred_element_type=jnp.float32)  11 us
    all_to_all x1, waiting for transfers between devices, body(): lax.all_to_all(halves.reshape(ep_count, count, part_width).astype(jnp.bfl...  10.8 us
    dot_general x1, matrix products, body(): total = jnp.dot(activity, down_piece, preferred_element_type=jnp.float32)  9.19 us
    all_to_all x1, starting transfers between devices, body(): lax.all_to_all(halves.reshape(ep_count, count, part_width).astype(jnp.bfl...  8.6 us
    all_to_all x2, blocking collectives, sent_and_summed(): lax.all_to_all(cut_along(shard, dim, devices), axis, 0, 0, tiled=True)  7.95 us
  transfers between devices with their start and end apart: 4, of which 3 were waited for; matrix products, arithmetic and copies ran while one was open for 11% of the time, Pallas kernels for 0%

profile of v1, /device:TPU:0, one launch (start us, length us, event | category | flops | bytes accessed | tf_op | source)
XLA Modules:
  0.0 294.3 jit_solution(6559463762706027675)
XLA Ops:
  7.2 0.8 copy.57
  8.0 0.8 copy.58
  8.8 1.5 concatenate.6
  10.4 1.8 pad_maximum_fusion
  12.3 2.3 stack.2
  14.6 11.5 %all-to-all-start = ((bf16[64,512,32]{1,2,0:T(8,128)(2,1)}), bf16[64,512,32]{1,2,0:T(8,128)(2,1)S(1)}, u32[]{:S(2)}, u32[]{:S(2)}) async-start(bf16[64,512,32]{1,2,0:T(8,128)(2,1)} %stack.2), calls=%async_computation | async-start | bytes 4194304 | tf_op jit(solution)/shard_map/all_to_all | solution.py:151
  26.7 84.1 %all-gather.3.cloned.1.call-done = bf16[2048,2056]{1,0:T(8,128)(2,1)} async-done(((bf16[32,2056]{1,0:T(8,128)(2,1)}), bf16[2048,2056]{1,0:T(8,128)(2,1)}) %all-gather.3.cloned.1.call-update) | async-done | bytes 8421392 | tf_op jit(solution)/shard_map/all_gather | solution.py:14
  110.8 1.3 fusion.94
  112.1 1.7 subtract_exponential_fusion.1
  113.9 2.0 fusion.58
  116.0 2.0 fusion.67
  118.1 2.0 fusion.70
  120.1 2.0 fusion.88
  122.3 3.2 %multiply_add_fusion = f32[16,4,128,128]{3,2,1,0:T(8,128)S(1)} fusion(f32[16,4,128,128]{3,2,1,0:T(8,128)} %param.32, f32[16,4,128]{2,1,0:T(4,128)S(1)} %mul.168, f32[16,4,128]{2,1,0:T(4,128)S(1)} %broadcast_multiply_fusion, f32[16,4]{1,0:T(8,128)S(1)} %copy.59), kind=kLoop, calls=%fused_computation.12 | loop fusion | flops 3145728 | bytes 8454400 | tf_op jit(solution)/shard_map/add | solution.py:72
  125.5 2.0 copy-done
  127.5 1.2 fusion.149
  128.9 0.6 convolution_convert_fusion.1
  129.6 3.8 %all_to_all.30 = bf16[2,16,2048]{2,1,0:T(8,128)(2,1)S(1)} all-to-all(bf16[2,16,2048]{2,1,0:T(8,128)(2,1)S(1)} %broadcast_in_dim.10), channel_id=1, replica_groups=mesh['ep'=64,'tp'=2] {'tp'}, dimensions={0} | all-to-all | bytes 262144 | tf_op jit(solution)/shard_map/all_to_all | solution.py:20
  133.7 0.4 convolution_convert_fusion
  134.1 0.5 copy.63
  134.6 26.4 %all_to_all.31 = bf16[64,2,2048]{2,1,0:T(2,128)(2,1)S(1)} all-to-all(bf16[64,2,2048]{2,1,0:T(2,128)(2,1)S(1)} %copy.63), channel_id=1, replica_groups=mesh['ep'=64,'tp'=2] {'ep'}, dimensions={0} | all-to-all | bytes 1048576 | tf_op jit(solution)/shard_map/all_to_all | solution.py:177
  161.2 3.0 %fusion.37 = f32[128,1024]{1,0:T(8,128)S(1)} fusion(bf16[128,2048]{1,0:T(8,128)(2,1)S(1)} %reshape.107, bf16[1,2048,1024]{2,1,0:T(8,128)(2,1)} %param.39), kind=kOutput, calls=%fused_computation.28 | convolution fusion | flops 537001984 | bytes 5242880 | tf_op jit(solution)/shard_map/dot_general | solution.py:86
  164.2 5.0 %fusion.12 = bf16[128,2048]{1,0:T(8,128)(2,1)S(1)} fusion(bf16[1,1024,2048]{2,1,0:T(8,128)(2,1)} %param.41, f32[128,1024]{1,0:T(8,128)S(1)} %fusion.37, bf16[128,2048]{1,0:T(8,128)(2,1)S(1)} %reshape.107, bf16[1,2048,1024]{2,1,0:T(8,128)(2,1)} %param.40), kind=kOutput, calls=%fused_computation.13 | convolution fusion | flops 1075183616 | bytes 9961472 | tf_op jit(solution)/shard_map/dot_general | solution.py:89
  169.3 4.2 %all_to_all.32 = bf16[2,128,1024]{2,1,0:T(8,128)(2,1)S(1)} all-to-all(bf16[2,128,1024]{2,1,0:T(8,128)(2,1)S(1)} %bitcast.71), channel_id=1, replica_groups=mesh['ep'=64,'tp'=2] {'tp'}, dimensions={0} | all-to-all | bytes 1048576 | tf_op jit(solution)/shard_map/all_to_all | solution.py:37
  173.5 0.8 convert_element_type.114
  174.4 74.0 %all-gather.5.cloned.1.call-done = bf16[2048,6144]{1,0:T(8,128)(2,1)} async-done(((bf16[32,6144]{1,0:T(8,128)(2,1)}), bf16[2048,6144]{1,0:T(8,128)(2,1)}) %all-gather.5.cloned.1.call-update) | async-done | bytes 25165840 | tf_op jit(solution)/shard_map/all_gather | solution.py:14
  248.4 5.6 %fusion.4 = f32[16,2048]{1,0:T(8,128)S(1)} fusion(bf16[16,2048]{1,0:T(8,128)(2,1)S(1)} %multiply_convert_fusion, bf16[2048,6144]{1,0:T(8,128)(2,1)} %all-gather.5.cloned.1.call-done), kind=kOutput, calls=%fused_computation.4 | convolution fusion | flops 134217728 | bytes 8585216 | tf_op jit(solution)/shard_map/td,fd->tf/dot_general | solution.py:192
  254.0 9.2 %fusion.21 = bf16[16,2048]{1,0:T(8,128)(2,1)S(1)} fusion(bf16[2048,6144]{1,0:T(8,128)(2,1)} %all-gather.5.cloned.1.call-done, bf16[16,2048]{1,0:T(8,128)(2,1)S(1)} %multiply_convert_fusion, f32[16,2048]{1,0:T(8,128)S(1)} %fusion.4), kind=kOutput, calls=%fused_computation.17 | convolution fusion | flops 268664832 | bytes 17039360 | tf_op jit(solution)/shard_map/dot_general | solution.py:197
  263.2 3.8 %all_to_all.33 = bf16[2,16,1024]{2,1,0:T(8,128)(2,1)S(1)} all-to-all(bf16[2,16,1024]{2,1,0:T(8,128)(2,1)S(1)} %bitcast.75), channel_id=1, replica_groups=mesh['ep'=64,'tp'=2] {'tp'}, dimensions={0} | all-to-all | bytes 131072 | tf_op jit(solution)/shard_map/all_to_all | solution.py:37
  267.0 8.6 %all-to-all-start.4 = ((bf16[64,2,1024]{2,1,0:T(2,128)(2,1)}), bf16[64,2,1024]{2,1,0:T(2,128)(2,1)S(1)}, u32[]{:S(2)}, u32[]{:S(2)}) async-start(bf16[64,2,1024]{2,1,0:T(2,128)(2,1)} %convert_element_type.114), calls=%async_computation.4 | async-start | bytes 524288 | tf_op jit(solution)/shard_map/all_to_all | solution.py:183
  275.8 10.8 %all-to-all-done.4 = bf16[64,2,1024]{2,1,0:T(2,128)(2,1)S(1)} async-done(((bf16[64,2,1024]{2,1,0:T(2,128)(2,1)}), bf16[64,2,1024]{2,1,0:T(2,128)(2,1)S(1)}, u32[]{:S(2)}, u32[]{:S(2)}) %all-to-all-start.4) | async-done | bytes 262176 | tf_op jit(solution)/shard_map/all_to_all | solution.py:183
  286.5 0.9 fusion.54
  (58 shorter events, 2.0 us)
Async XLA Ops:
  7.2 19.0 %copy-start.3 = (s32[16,4]{0,1:T(4,128)S(1)}, s32[16,4]{0,1:T(4,128)}, u32[]{:S(2)}) copy-start(s32[16,4]{0,1:T(4,128)} %param.37) | copy-start | bytes 772
  7.2 19.4 %copy-start.1 = (bf16[16,2048]{1,0:T(8,128)(2,1)S(1)}, bf16[16,2048]{1,0:T(8,128)(2,1)}, u32[]{:S(2)}) copy-start(bf16[16,2048]{1,0:T(8,128)(2,1)} %param.23) | copy-start | bytes 196612
  7.2 103.7 %copy-start.8 = (f32[2048]{0:T(1024)S(1)}, f32[2048]{0:T(1024)}, u32[]{:S(2)}) copy-start(f32[2048]{0:T(1024)} %param.24) | copy-start | bytes 24580
  7.2 103.6 %all-gather.3.cloned.1.call-start = ((), (), s32[]{:S(2)}) async-start(), calls=%async_computation.6 | async-start | bytes 9052160 | tf_op jit(solution)/shard_map/all_gather | solution.py:14
  10.4 101.8 %copy-start.9 = (f32[16,4]{0,1:T(4,128)S(1)}, f32[16,4]{0,1:T(4,128)}, u32[]{:S(2)}) copy-start(f32[16,4]{0,1:T(4,128)} %param.33) | copy-start | bytes 772
  10.4 101.8 %copy-start.10 = (f32[4]{0:T(128)S(1)}, f32[4]{0:T(128)}, u32[]{:S(2)}) copy-start(f32[4]{0:T(128)} %param.31) | copy-start | bytes 52
  10.4 238.0 %all-gather.5.cloned.1.call-start = ((), (), s32[]{:S(2)}) async-start(), calls=%async_computation.7 | async-start | bytes 25559040 | tf_op jit(solution)/shard_map/all_gather | solution.py:14
  14.6 114.3 %all-to-all-start = ((bf16[64,512,32]{1,2,0:T(8,128)(2,1)}), bf16[64,512,32]{1,2,0:T(8,128)(2,1)S(1)}, u32[]{:S(2)}, u32[]{:S(2)}) async-start(bf16[64,512,32]{1,2,0:T(8,128)(2,1)} %stack.2), calls=%async_computation | async-start | bytes 4194304 | tf_op jit(solution)/shard_map/all_to_all | solution.py:151
  113.8 8.3 %copy-start.5 = (f32[16,4]{0,1:T(4,128)}, f32[16,4]{0,1:T(4,128)S(1)}, u32[]{:S(2)}) copy-start(f32[16,4]{0,1:T(4,128)S(1)} %get-tuple-element.6) | copy-start | bytes 772
  125.5 2.0 copy-start
  127.5 1.3 copy-start.4
  127.5 6.1 %copy-start.2 = (f32[2048]{0:T(1024)S(1)}, f32[2048]{0:T(1024)}, u32[]{:S(2)}) copy-start(f32[2048]{0:T(1024)} %param.36) | copy-start | bytes 24580
  254.0 21.6 %copy-start.6 = (f32[2048]{0:T(1024)S(1)}, f32[2048]{0:T(1024)}, u32[]{:S(2)}) copy-start(f32[2048]{0:T(1024)} %param.45) | copy-start | bytes 24580
  254.0 21.6 %copy-start.7 = (f32[16,4]{0,1:T(4,128)S(1)}, f32[16,4]{0,1:T(4,128)}, u32[]{:S(2)}) copy-start(f32[16,4]{0,1:T(4,128)} %param.38) | copy-start | bytes 772
  267.0 19.5 %all-to-all-start.4 = ((bf16[64,2,1024]{2,1,0:T(2,128)(2,1)}), bf16[64,2,1024]{2,1,0:T(2,128)(2,1)S(1)}, u32[]{:S(2)}, u32[]{:S(2)}) async-start(bf16[64,2,1024]{2,1,0:T(2,128)(2,1)} %convert_element_type.114), calls=%async_computation.4 | async-start | bytes 524288 | tf_op jit(solution)/shard_map/all_to_all | solution.py:183
Sparse Core Ops, SparseCore 0:
  11.4 99.4 all-gather.2
  113.6 134.7 all-gather.4
